TPU v7x, 256 devices: a 4x2x16 block of a 4x16x16 slice. The times are simulated.
256 devices in a mesh: grp: 2 (over y), fs: 16 (over z), tp: 8 (over x, core).
Axes of the slice: x: 4, y: 2, z: 16, core: 2. Of those that a mesh axis runs over, the one named last changes fastest.
The devices are a block of a 4x16x16 slice.
Arguments:
- layer_input: bfloat16 [12288, 2048], P(('grp', 'fs'), 'tp'), parts along dimension 0, may hold values from -6 to 6
- first_gain: bfloat16 [1, 2048], P(None, 'tp'), may hold values from 0.099609375 to 1.8984375
- ffn_gate_w: bfloat16 [2048, 6144], P('fs', 'tp'), may hold values from -0.125 to 0.125
- ffn_up_w: bfloat16 [2048, 6144], P('fs', 'tp'), may hold values from -0.125 to 0.125
- ffn_down_w: bfloat16 [6144, 2048], P('tp', 'fs'), may hold values from -0.078125 to 0.078125
- mixer_gain: bfloat16 [1, 2048], P(None, 'tp'), may hold values from 0.099609375 to 1.8984375
- pool_in_w: bfloat16 [2048, 1024], P('fs', 'tp'), may hold values from -0.125 to 0.125
- mixer_gate_w: bfloat16 [2048, 2048], P('fs', 'tp'), may hold values from -0.125 to 0.125
- group_mix_w: bfloat16 [8, 128, 128], P('tp'), may hold values from -0.5 to 0.5
- pool_scale: float32 [1, 1024], P(None, 'tp'), may hold values from 0.1 to 1.9
- mixer_out_w: bfloat16 [1024, 2048], P('tp', 'fs'), may hold values from -0.1875 to 0.1875
- second_gain: bfloat16 [1, 2048], P(None, 'tp'), may hold values from 0.099609375 to 1.8984375
Outputs:
- layer_output: bfloat16 [12288, 2048], P(('grp', 'fs'), 'tp'), parts along dimension 0
There are 2 independent parts, one for each index of `grp`. A program takes and returns all parts, laid end to end along the dimension named above; an argument that names none is the same for every part. Nothing has to cross between parts.
All inputs are finite; a program needn't handle non-finite values.
Results may differ from a plain program's by a relative error of at most 0.015.
Values may be sent and summed in bfloat16 or wider, within the bound.
A program may use at most 64 MiB of HBM per device.

v0:
```python
import jax
import jax.numpy as jnp
from jax import lax
from jax.sharding import Mesh
from jax.sharding import PartitionSpec as P

TP = ("tp_0", "tp_1")


def from_everyone(value, axis):
    length = lax.axis_size(axis)
    return lax.all_to_all(
        jnp.broadcast_to(value[None], (length, *value.shape)), axis, 0, 0, tiled=True
    )


def joined_along(tiles, dim):
    shape = list(tiles.shape[1:])
    shape[dim] *= tiles.shape[0]
    return jnp.moveaxis(tiles, 0, dim).reshape(shape)


def whole_of(value, axes, dim):
    far, near = axes
    initial = from_everyone(value, far)
    tiles = jnp.swapaxes(from_everyone(initial, near), 0, 1)
    return joined_along(tiles.reshape(-1, *value.shape), dim)


def in_one_piece(arrays, axis, dim, along):
    widths = [a.shape[along] for a in arrays]
    both = jnp.concatenate(arrays, axis=along)
    filled = whole_of(both, axis, dim)
    return tuple(jnp.split(filled, [sum(widths[:k]) for k in range(1, len(widths))], axis=along))


def in_blocks(value, dim, length):
    before, after = (value.shape[:dim], value.shape[dim + 1 :])
    return jnp.moveaxis(value.reshape(*before, length, -1, *after), dim, 0)


def summed_on_arrival(value, axis, dim):
    tiles = in_blocks(value, dim, lax.axis_size(axis))
    arrived = lax.all_to_all(tiles, axis, split_axis=0, concat_axis=0, tiled=True)
    return arrived.astype(jnp.float32).sum(axis=0)


def sent_together(arrays, axis, dim, along):
    ends, at = ([], 0)
    for a in arrays[:-1]:
        at += a.shape[along]
        ends.append(at)
    both = jnp.concatenate(arrays, axis=along)
    return tuple(jnp.split(lax.all_gather(both, axis, axis=dim, tiled=True), ends, axis=along))


def gather_directly(value, axis, dim):
    return joined_along(from_everyone(value, axis), dim)


def norm_rows(values, gain):
    gathered, gain_whole = in_one_piece((values, gain), ("tp_0", "tp_1"), 1, 0)
    widened = gathered.astype(jnp.float32)
    scaled = (widened * gain_whole.astype(jnp.float32)).astype(jnp.bfloat16)
    factor = lax.rsqrt(jnp.mean(widened * widened, axis=1, keepdims=True) + 1e-06)
    return (scaled, factor)


def column_sums(partial_value):
    return summed_on_arrival(partial_value.astype(jnp.bfloat16), TP, 1)


def add_pair(scaled, pieces):
    first_sum = jnp.dot(scaled, pieces[0], preferred_element_type=jnp.float32)
    second_sum = jnp.dot(scaled, pieces[1], preferred_element_type=jnp.float32)
    return (first_sum, second_sum)


def per_device(
    layer_input,
    first_gain,
    ffn_gate_w,
    ffn_up_w,
    ffn_down_w,
    mixer_gain,
    pool_in_w,
    mixer_gate_w,
    group_mix_w,
    pool_scale,
    mixer_out_w,
    second_gain,
):
    row_count = layer_input.shape[0]
    gate_whole, up_whole = sent_together((ffn_gate_w, ffn_up_w), "fs", 0, 1)
    down_whole = lax.all_gather(ffn_down_w, "fs", axis=1, tiled=True)

    def feed_forward(values, gain):
        scaled, factor = norm_rows(values, gain)
        gate_pre = factor * jnp.dot(scaled, gate_whole, preferred_element_type=jnp.float32)
        up_pre = factor * jnp.dot(scaled, up_whole, preferred_element_type=jnp.float32)
        hidden = (jax.nn.silu(gate_pre) * up_pre).astype(jnp.bfloat16)
        return jnp.dot(hidden, down_whole, preferred_element_type=jnp.float32)

    first = (
        layer_input.astype(jnp.float32) + 0.5 * column_sums(feed_forward(layer_input, first_gain))
    ).astype(jnp.bfloat16)
    scaled, factor = norm_rows(first, mixer_gain)
    pool_sum, gate_sum = add_pair(scaled, sent_together((pool_in_w, mixer_gate_w), "fs", 0, 1))
    pool_pre = (factor * pool_sum).astype(jnp.bfloat16)
    gate_logit = factor * gate_sum
    group_count = group_mix_w.shape[0]
    group_width = group_mix_w.shape[1]
    first_group = lax.axis_index(TP) * group_count
    values = pool_pre.astype(jnp.float32).reshape(row_count, group_count, group_width)
    running = jnp.cumsum(values, axis=0)
    positions = jnp.arange(row_count, dtype=jnp.int32)
    windows = 2 ** (1 + (first_group + jnp.arange(group_count, dtype=jnp.int32)) % 4)
    chosen = jnp.zeros_like(values)
    for span in (2, 4, 8, 16):
        lagged = jnp.pad(running, ((span, 0), (0, 0), (0, 0)))[:row_count]
        counts = jnp.minimum(positions + 1, span).astype(jnp.float32)[:, None, None]
        means = (running - lagged) / counts
        chosen = jnp.where((windows == span)[None, :, None], means, chosen)
    trail = (chosen - values).astype(jnp.bfloat16)
    mixed = jnp.einsum("tgc,gcd->tgd", trail, group_mix_w, preferred_element_type=jnp.float32)
    pooled = (mixed.reshape(row_count, group_count * group_width) * pool_scale).astype(jnp.bfloat16)
    lifted = column_sums(
        jnp.dot(pooled, gather_directly(mixer_out_w, "fs", 1), preferred_element_type=jnp.float32)
    )
    second = (first.astype(jnp.float32) + jax.nn.sigmoid(gate_logit) * lifted).astype(jnp.bfloat16)
    result = second.astype(jnp.float32) + 0.5 * column_sums(feed_forward(second, second_gain))
    return result.astype(jnp.bfloat16)


def solution(mesh):
    finer = Mesh(
        mesh.devices.reshape(mesh.shape["grp"], mesh.shape["fs"], 4, 2),
        ("grp", "fs", "tp_0", "tp_1"),
    )
    return jax.shard_map(
        per_device,
        mesh=finer,
        in_specs=(
            P(("grp", "fs"), TP),
            P(None, TP),
            P("fs", TP),
            P("fs", TP),
            P(TP, "fs"),
            P(None, TP),
            P("fs", TP),
            P("fs", TP),
            P(TP, None, None),
            P(None, TP),
            P(TP, "fs"),
            P(None, TP),
        ),
        out_specs=P(("grp", "fs"), TP),
        check_vma=False,
    )
```

profile of v0, /device:TPU:33, one launch (start us, length us, event | category | flops | bytes accessed | tf_op | source)
XLA Modules:
  0.0 387.3 jit_solution(81376959434211735)
XLA Ops:
  6.6 1.8 pad_maximum_fusion
  8.5 0.7 all-gather.6.cloned.1.call-update
  9.2 1.0 pad_maximum_fusion.1
  10.3 13.3 %all_to_all.50 = bf16[4,385,256]{2,1,0:T(8,128)(2,1)S(1)} all-to-all(bf16[4,385,256]{2,1,0:T(8,128)(2,1)S(1)} %broadcast_in_dim.91), channel_id=1, replica_groups=mesh['grp'=2,'fs'=16,'tp_0'=4,'tp_1'=2] {'tp_0'}, dimensions={0} | all-to-all | bytes 1576960 | tf_op jit(solution)/shard_map/all_to_all | solution.py:12
  23.9 0.4 broadcast_in_dim.92
  24.3 23.7 %all_to_all.51 = bf16[2,4,385,256]{3,1,2,0:T(4,128)(2,1)S(1)} all-to-all(bf16[2,4,385,256]{3,1,2,0:T(4,128)(2,1)S(1)} %broadcast_in_dim.92), channel_id=1, replica_groups=mesh['grp'=2,'fs'=16,'tp_0'=4,'tp_1'=2] {'tp_1'}, dimensions={0} | all-to-all | bytes 3153920 | tf_op jit(solution)/shard_map/all_to_all | solution.py:12
  48.2 1.9 slice_convert_fusion.2
  50.2 3.6 copy.35
  54.1 2.3 fusion.2
  56.4 48.7 %all-gather.4.cloned.1.call-done = bf16[2048,1536]{1,0:T(8,128)(2,1)} async-done(((bf16[128,1536]{1,0:T(8,128)(2,1)}), bf16[2048,1536]{1,0:T(8,128)(2,1)}) %all-gather.4.cloned.1.call-update) | async-done | bytes 6291472 | tf_op jit(solution)/shard_map/all_gather | solution.py:54
  105.1 4.3 %fusion.11 = f32[384,768]{1,0:T(8,128)} fusion(bf16[384,2048]{0,1:T(8,128)(2,1)S(1)} %fusion.2, bf16[2048,1536]{1,0:T(8,128)(2,1)} %all-gather.4.cloned.1.call-done, f32[384]{0:T(512)S(1)} %add_rsqrt_fusion.2), kind=kOutput, calls=%fused_computation.29 | convolution fusion | flops 1208254464 | bytes 5899776 | tf_op jit(solution)/shard_map/dot_general | solution.py:99
  109.4 71.1 %all-gather.6.cloned.1.call-done = bf16[768,2048]{1,0:T(8,128)(2,1)} async-done(((bf16[768,128]{1,0:T(8,128)(2,1)}), bf16[768,2048]{1,0:T(8,128)(2,1)}) %all-gather.6.cloned.1.call-update) | async-done | bytes 3145744 | tf_op jit(solution)/shard_map/all_gather | solution.py:95
  180.5 6.4 %convolution_convert_fusion.1 = bf16[384,2048]{1,0:T(8,128)(2,1)S(1)} fusion(bf16[768,2048]{1,0:T(8,128)(2,1)} %all-gather.6.cloned.1.call-done, bf16[384,2048]{0,1:T(8,128)(2,1)S(1)} %fusion.2, bf16[2048,1536]{1,0:T(8,128)(2,1)} %all-gather.4.cloned.1.call-done, f32[384,768]{1,0:T(8,128)} %fusion.11, f32[384]{0:T(512)S(1)} %add_rsqrt_fusion.2), kind=kOutput, calls=%fused_computation.13 | convolution fusion | flops 2418769920 | bytes 10618368 | tf_op jit(solution)/shard_map/dot_general | solution.py:102
  186.9 1.3 copy.58
  188.1 15.3 %all-to-all-start.2 = ((bf16[8,384,256]{2,1,0:T(8,128)(2,1)}), bf16[8,384,256]{2,1,0:T(8,128)(2,1)S(1)}, u32[]{:S(2)}, u32[]{:S(2)}) async-start(bf16[8,384,256]{2,1,0:T(8,128)(2,1)} %bitcast.111), calls=%async_computation.2 | async-start | bytes 3145728 | tf_op jit(solution)/shard_map/all_to_all | solution.py:44
  203.5 0.7 pad_maximum_fusion.4
  204.2 19.8 %all-to-all-done.2 = bf16[8,384,256]{2,1,0:T(8,128)(2,1)S(1)} async-done(((bf16[8,384,256]{2,1,0:T(8,128)(2,1)}), bf16[8,384,256]{2,1,0:T(8,128)(2,1)S(1)}, u32[]{:S(2)}, u32[]{:S(2)}) %all-to-all-start.2) | async-done | bytes 1572896 | tf_op jit(solution)/shard_map/all_to_all | solution.py:44
  224.4 0.9 broadcast_in_dim.93
  225.3 3.6 all-to-all-start.3
  229.1 11.3 %all-to-all-done.3 = bf16[4,385,256]{2,1,0:T(8,128)(2,1)S(1)} async-done(((bf16[4,385,256]{2,1,0:T(8,128)(2,1)}), bf16[4,385,256]{2,1,0:T(8,128)(2,1)S(1)}, u32[]{:S(2)}, u32[]{:S(2)}) %all-to-all-start.3) | async-done | bytes 788512 | tf_op jit(solution)/shard_map/all_to_all | solution.py:12
  240.7 0.4 broadcast_in_dim.94
  241.1 6.5 %all_to_all.52 = bf16[2,4,385,256]{3,1,2,0:T(4,128)(2,1)S(1)} all-to-all(bf16[2,4,385,256]{3,1,2,0:T(4,128)(2,1)S(1)} %broadcast_in_dim.94), channel_id=1, replica_groups=mesh['grp'=2,'fs'=16,'tp_0'=4,'tp_1'=2] {'tp_1'}, dimensions={0} | all-to-all | bytes 3153920 | tf_op jit(solution)/shard_map/all_to_all | solution.py:12
  247.6 0.9 broadcast_in_dim.104
  248.5 7.0 %all-to-all-start.5 = ((bf16[16,128,128]{1,2,0:T(8,128)(2,1)}), bf16[16,128,128]{1,2,0:T(8,128)(2,1)}, u32[]{:S(2)}, u32[]{:S(2)}) async-start(bf16[16,128,128]{1,2,0:T(8,128)(2,1)} %broadcast_in_dim.104), calls=%async_computation.5 | async-start | bytes 1048576 | tf_op jit(solution)/shard_map/all_to_all | solution.py:12
  255.7 1.9 slice_convert_fusion.1
  257.6 3.5 copy.39
  261.5 2.2 fusion.1
  263.8 3.6 all-gather.8.cloned.1.call-done
  267.4 1.6 fusion.47
  269.1 0.7 copy-done.6
  270.0 0.7 fusion.73
  270.7 10.8 %all-to-all-done.5 = bf16[16,128,128]{1,2,0:T(8,128)(2,1)} async-done(((bf16[16,128,128]{1,2,0:T(8,128)(2,1)}), bf16[16,128,128]{1,2,0:T(8,128)(2,1)}, u32[]{:S(2)}, u32[]{:S(2)}) %all-to-all-start.5) | async-done | bytes 524320 | tf_op jit(solution)/shard_map/all_to_all | solution.py:12
  281.5 2.4 convolution_convert_fusion.2
  284.0 31.3 %all_to_all.53 = bf16[8,384,256]{2,1,0:T(8,128)(2,1)S(1)} all-to-all(bf16[8,384,256]{2,1,0:T(8,128)(2,1)S(1)} %bitcast.125), channel_id=1, replica_groups=mesh['grp'=2,'fs'=16,'tp_0'=4,'tp_1'=2] {'tp_0','tp_1'}, dimensions={0} | all-to-all | bytes 3145728 | tf_op jit(solution)/shard_map/all_to_all | solution.py:44
  315.5 1.2 copy-done.12
  316.7 0.7 fusion.41
  317.4 0.6 copy-done.4
  318.1 13.9 %all_to_all.54 = bf16[4,385,256]{2,1,0:T(8,128)(2,1)S(1)} all-to-all(bf16[4,385,256]{2,1,0:T(8,128)(2,1)S(1)} %broadcast_in_dim.105), channel_id=1, replica_groups=mesh['grp'=2,'fs'=16,'tp_0'=4,'tp_1'=2] {'tp_0'}, dimensions={0} | all-to-all | bytes 1576960 | tf_op jit(solution)/shard_map/all_to_all | solution.py:12
  332.3 0.4 broadcast_in_dim.106
  332.7 6.5 %all_to_all.55 = bf16[2,4,385,256]{3,1,2,0:T(4,128)(2,1)S(1)} all-to-all(bf16[2,4,385,256]{3,1,2,0:T(4,128)(2,1)S(1)} %broadcast_in_dim.106), channel_id=1, replica_groups=mesh['grp'=2,'fs'=16,'tp_0'=4,'tp_1'=2] {'tp_1'}, dimensions={0} | all-to-all | bytes 3153920 | tf_op jit(solution)/shard_map/all_to_all | solution.py:12
  339.5 1.9 slice_convert_fusion
  341.8 2.4 copy.46
  344.6 1.2 copy-done.2
  345.7 3.3 fusion.14
  349.1 6.5 %convolution_convert_fusion = bf16[384,2048]{1,0:T(8,128)(2,1)S(1)} fusion(bf16[768,2048]{1,0:T(8,128)(2,1)} %all-gather.6.cloned.1.call-done, bf16[384,2048]{0,1:T(8,128)(2,1)} %copy-done.2, bf16[2048,1536]{1,0:T(8,128)(2,1)} %all-gather.4.cloned.1.call-done, f32[384,768]{1,0:T(8,128)S(1)} %fusion.14, f32[384]{0:T(512)S(1)} %add_rsqrt_fusion), kind=kOutput, calls=%fused_computation.12 | convolution fusion | flops 2418769920 | bytes 10618368 | tf_op jit(solution)/shard_map/dot_general | solution.py:102
  355.7 23.4 %all_to_all.56 = bf16[8,384,256]{2,1,0:T(8,128)(2,1)S(1)} all-to-all(bf16[8,384,256]{2,1,0:T(8,128)(2,1)S(1)} %bitcast.126), channel_id=1, replica_groups=mesh['grp'=2,'fs'=16,'tp_0'=4,'tp_1'=2] {'tp_0','tp_1'}, dimensions={0} | all-to-all | bytes 3145728 | tf_op jit(solution)/shard_map/all_to_all | solution.py:44
  379.3 0.7 copy-done.5
  380.0 0.7 add_convert_fusion
  (63 shorter events, 4.8 us)
Async XLA Ops:
  6.5 275.0 %copy-start = (bf16[1,128,128]{2,1,0:T(8,128)(2,1)S(1)}, bf16[1,128,128]{2,1,0:T(8,128)(2,1)}, u32[]{:S(2)}) copy-start(bf16[1,128,128]{2,1,0:T(8,128)(2,1)} %param.20) | copy-start | bytes 98308
  6.6 98.6 %all-gather.4.cloned.1.call-start = ((), (), s32[]{:S(2)}) async-start(), calls=%async_computation.10 | async-start | bytes 6684672 | tf_op jit(solution)/shard_map/all_gather | solution.py:54
  8.4 172.1 %all-gather.6.cloned.1.call-start = ((), (), s32[]{:S(2)}) async-start(), calls=%async_computation.11 | async-start | bytes 3342336 | tf_op jit(solution)/shard_map/all_gather | solution.py:95
  188.1 15.4 %copy-start.7 = (bf16[128,256]{1,0:T(8,128)(2,1)S(1)}, bf16[128,256]{1,0:T(8,128)(2,1)}, u32[]{:S(2)}) copy-start(bf16[128,256]{1,0:T(8,128)(2,1)} %param.19) | copy-start | bytes 196612
  188.1 15.4 %copy-start.9 = (bf16[128,128]{1,0:T(8,128)(2,1)S(1)}, bf16[128,128]{1,0:T(8,128)(2,1)}, u32[]{:S(2)}) copy-start(bf16[128,128]{1,0:T(8,128)(2,1)} %param.18) | copy-start | bytes 98308
  188.1 35.9 %all-to-all-start.2 = ((bf16[8,384,256]{2,1,0:T(8,128)(2,1)}), bf16[8,384,256]{2,1,0:T(8,128)(2,1)S(1)}, u32[]{:S(2)}, u32[]{:S(2)}) async-start(bf16[8,384,256]{2,1,0:T(8,128)(2,1)} %bitcast.111), calls=%async_computation.2 | async-start | bytes 3145728 | tf_op jit(solution)/shard_map/all_to_all | solution.py:44
  203.4 20.8 %copy-start.3 = (bf16[384,256]{1,0:T(8,128)(2,1)S(1)}, bf16[384,256]{1,0:T(8,128)(2,1)}, u32[]{:S(2)}) copy-start(bf16[384,256]{1,0:T(8,128)(2,1)} %param.12) | copy-start | bytes 589828
  203.4 20.9 %copy-start.10 = (bf16[1,256]{1,0:T(2,128)(2,1)S(1)}, bf16[1,256]{1,0:T(2,128)(2,1)}, u32[]{:S(2)}) copy-start(bf16[1,256]{1,0:T(2,128)(2,1)} %param.17) | copy-start | bytes 1540
  203.4 64.0 %all-gather.8.cloned.1.call-start = ((), (), s32[]{:S(2)}) async-start(), calls=%async_computation.12 | async-start | bytes 1671168 | tf_op jit(solution)/shard_map/all_gather | solution.py:54
  224.3 4.6 %copy-start.8 = (bf16[128,128]{1,0:T(8,128)(2,1)S(1)}, bf16[128,128]{1,0:T(8,128)(2,1)}, u32[]{:S(2)}) copy-start(bf16[128,128]{1,0:T(8,128)(2,1)} %param.22) | copy-start | bytes 98308
  225.3 15.1 %all-to-all-start.3 = ((bf16[4,385,256]{2,1,0:T(8,128)(2,1)}), bf16[4,385,256]{2,1,0:T(8,128)(2,1)S(1)}, u32[]{:S(2)}, u32[]{:S(2)}) async-start(bf16[4,385,256]{2,1,0:T(8,128)(2,1)} %broadcast_in_dim.93), calls=%async_computation.3 | async-start | bytes 1605632 | tf_op jit(solution)/shard_map/all_to_all | solution.py:12
  248.5 33.0 %all-to-all-start.5 = ((bf16[16,128,128]{1,2,0:T(8,128)(2,1)}), bf16[16,128,128]{1,2,0:T(8,128)(2,1)}, u32[]{:S(2)}, u32[]{:S(2)}) async-start(bf16[16,128,128]{1,2,0:T(8,128)(2,1)} %broadcast_in_dim.104), calls=%async_computation.5 | async-start | bytes 1048576 | tf_op jit(solution)/shard_map/all_to_all | solution.py:12
  269.1 0.7 copy-start.6
  269.1 12.4 %copy-start.13 = (f32[1,128]{1,0:T(1,128)S(1)}, f32[1,128]{1,0:T(1,128)}, u32[]{:S(2)}) copy-start(f32[1,128]{1,0:T(1,128)} %param.21) | copy-start | bytes 1540
  315.3 1.4 copy-start.12
  316.7 0.7 copy-start.11
  317.4 0.7 copy-start.4
  344.6 1.2 copy-start.2
  355.7 25.1 %copy-start.1 = (bf16[1,128,128]{2,1,0:T(8,128)(2,1)S(1)}, bf16[1,128,128]{2,1,0:T(8,128)(2,1)}, u32[]{:S(2)}) copy-start(bf16[1,128,128]{2,1,0:T(8,128)(2,1)} %param.20) | copy-start | bytes 98308
  379.1 0.9 copy-start.5
Sparse Core Ops, SparseCore 0:
  9.1 95.9 all-gather.3
  106.8 73.5 all-gather.5
  206.1 61.3 all-gather.7
where the time goes:
time: 388 us; the launch traced here: 387 us
  waiting for transfers between devices  166 us (43%)
  blocking collectives  119 us (31%)
  starting transfers between devices  26 us (7%)
  matrix products  25.2 us (6%)
  local copies, waits for them, and re-layouts  20.2 us (5%)
  other arithmetic  17.6 us (5%)
  between operations  13.6 us (4%)
    all_gather x1, waiting for transfers between devices, per_device(): down_whole = lax.all_gather(ffn_down_w, 'fs', axis=1, tiled=True)  71.1 us
    all_to_all x5, blocking collectives, from_everyone(): lax.all_to_all(jnp.broadcast_to(value[None], (length, *value.shape)), axi...  64 us
    all_to_all x2, blocking collectives, summed_on_arrival(): lax.all_to_all(tiles, axis, split_axis=0, concat_axis=0, tiled=True)  54.7 us
    all_gather x2, waiting for transfers between devices, sent_together(): lax.all_gather(both, axis, axis=dim, tiled=True)  52.3 us
    all_to_all x2, waiting for transfers between devices, from_everyone(): lax.all_to_all(jnp.broadcast_to(value[None], (length, *value.shape)), axi...  22.1 us
    all_to_all x1, waiting for transfers between devices, summed_on_arrival(): lax.all_to_all(tiles, axis, split_axis=0, concat_axis=0, tiled=True)  19.8 us
    all_to_all x1, starting transfers between devices, summed_on_arrival(): lax.all_to_all(tiles, axis, split_axis=0, concat_axis=0, tiled=True)  15.3 us
    dot_general x2, matrix products, feed_forward(): return jnp.dot(hidden, down_whole, preferred_element_type=jnp.float32)  12.9 us
  transfers between devices with their start and end apart: 6, of which 6 were waited for; matrix products, arithmetic and copies ran while one was open for 7% of the time, Pallas kernels for 0%

commit v1 on v0

v1 whole, which is shorter than its diff:
```python
import functools

import jax
import jax.numpy as jnp
from jax import lax
from jax.experimental import pallas as pl
from jax.experimental.pallas import tpu as pltpu
from jax.sharding import PartitionSpec as P

F32 = jnp.float32
BF16 = jnp.bfloat16
MESH = pl.DeviceIdType.MESH
EPS = 1e-06
RING_X = 4
NEAR = (2, 1, 3, 0)


def remote(src, dst, send, recv, device):
    return pltpu.make_async_remote_copy(
        src_ref=src, dst_ref=dst, send_sem=send, recv_sem=recv, device_id=device, device_id_type=MESH
    )


def kernel(
    n,
    x_hbm, g1_hbm, gate_hbm, up_hbm, down_hbm, gm_hbm, pin_hbm, mg_hbm, mix_hbm, ps_hbm, mo_hbm, g2_hbm,
    out_ref,
    xin, gains, mixw, pscale,
    wgu, wd, wpg, wo,
    acts, squares, factors, hidden, pre, first, second,
    pair_out, pair_in, turn_out, mid_in, last_in, kept, own,
    in_sem,
    zs_sem, zr_sem, ys_sem, yr_sem,
    ags_sem, agr_sem, sqs_sem, sqr_sem, rss_sem, rsr_sem,
):
    rows, width = x_hbm.shape
    half_rows = rows // 2
    tile = rows // 3
    kdim = gate_hbm.shape[0]
    third = gate_hbm.shape[1] // 3
    half_third = third // 2
    tpn = lax.axis_size("tp")
    features = tpn * width

    grp = lax.axis_index("grp")
    fs = lax.axis_index("fs")
    tp = lax.axis_index("tp")
    x = tp // 2
    core = tp % 2
    parity = grp % 2
    mine = 2 * parity
    other = 2 - mine

    z_right = {"fs": lax.rem(fs + 1, n)}
    z_left = {"fs": lax.rem(fs + n - 1, n)}
    z_dev = (z_right, z_left)
    y_dev = {"grp": grp + 1 - 2 * parity}
    partner = {"tp": tp + 1 - 2 * core}
    x_right = {"tp": lax.rem(tp + 2, tpn)}
    x_left = {"tp": lax.rem(tp + tpn - 2, tpn)}

    sent = []

    def begin(copy):
        copy.start()
        sent.append(copy)

    own_rows = pl.ds(pl.multiple_of(fs * kdim, kdim), kdim)
    local = []

    def fetch(src, dst):
        copy = pltpu.make_async_copy(src, dst, in_sem.at[len(local)])
        copy.start()
        local.append(copy)

    for q, ref in enumerate((gate_hbm, up_hbm)):
        for t in range(3):
            fetch(ref.at[:, pl.ds(t * third, third)], wgu.at[q, t, own_rows])
    fetch(x_hbm, xin)
    for k, ref in enumerate((g1_hbm, gm_hbm, g2_hbm)):
        fetch(ref, gains.at[k])
    early = len(local)
    for t in range(3):
        for h in range(2):
            fetch(down_hbm.at[pl.ds(t * third + h * half_third, half_third)], wd.at[t, h, fs])
    fetch(pin_hbm, wpg.at[0, own_rows])
    for t in range(2):
        fetch(mg_hbm.at[:, pl.ds(t * 128, 128)], wpg.at[1 + t, own_rows])
    fetch(mo_hbm, wo.at[fs])
    fetch(mix_hbm, mixw)
    fetch(ps_hbm, pscale)

    barrier = pltpu.get_barrier_semaphore()
    for dev in (z_right, z_left, y_dev):
        pl.semaphore_signal(barrier, inc=1, device_id=dev, device_id_type=MESH)
    for k in range(1, tpn):
        pl.semaphore_signal(barrier, inc=1, device_id={"tp": lax.rem(tp + k, tpn)}, device_id_type=MESH)
    pl.semaphore_wait(barrier, 3 + tpn - 1)

    def shard(d):
        return lax.rem(fs + n + d, n)

    def rows_of(s):
        return pl.ds(pl.multiple_of(s * kdim, kdim), kdim)

    def z_gate(s):
        return wgu.at[0, pl.ds(parity, 2), rows_of(s)]

    def z_up(s):
        return wgu.at[1, pl.ds(parity, 2), rows_of(s)]

    def z_down0(s):
        return wd.at[pl.ds(parity, 2), 0, s]

    def z_down1(s):
        return wd.at[pl.ds(parity, 2), 1, s]

    def z_pool(s):
        return wpg.at[pl.ds(parity, 2), rows_of(s)]

    def z_lift(s):
        return wo.at[s]

    half_n = n // 2
    chains = (z_gate, z_up, z_down0, z_down1, z_pool, z_lift)
    hops = ((half_n, half_n - 1), (half_n - 1, half_n)) * 3

    def y_gu(slot, s):
        return wgu.at[:, slot, rows_of(s)]

    def y_down(slot, s):
        return wd.at[slot, :, s]

    def y_pool(slot, s):
        return wpg.at[slot, rows_of(s)]

    y_kinds = (y_gu, y_down, y_pool)

    def z_send(k, direction, step):
        region = chains[k](shard(-step if direction == 0 else step))
        begin(remote(region, region, zs_sem.at[k, direction, step], zr_sem.at[k, direction, step], z_dev[direction]))

    def z_wait(k, direction, step):
        region = chains[k](shard(-step if direction == 0 else step))
        remote(
            region, region, zs_sem.at[k, direction, step - 1], zr_sem.at[k, direction, step - 1], z_dev[direction]
        ).wait_recv()
        if step < hops[k][direction]:
            z_send(k, direction, step)

    def y_send(kind, d):
        region = y_kinds[kind](mine, shard(d))
        begin(remote(region, region, ys_sem.at[kind, d % n], yr_sem.at[kind, d % n], y_dev))

    def y_wait_all(kind):
        for step in range(1, half_n + 1):
            for d in (-step, step) if step < half_n else (step,):
                region = y_kinds[kind](other, shard(d))
                remote(region, region, ys_sem.at[kind, d % n], yr_sem.at[kind, d % n], y_dev).wait_recv()

    def z_step(ks, kinds, step):
        for k in ks:
            for direction in range(2):
                if step <= hops[k][direction]:
                    z_wait(k, direction, step)
        for kind in kinds:
            for d in (-step, step) if step < half_n else (step,):
                y_send(kind, d)

    def ag_begin(i, values):
        wide = values.astype(F32)
        acts[i, tp] = (wide * gains[i].astype(F32)).astype(BF16)
        sq = wide * wide
        folded = sq[:, :128] + sq[:, 128:]
        squares[i, tp] = jnp.zeros((8, 128), F32)
        for r in range(3):
            squares[i, tp, r:r + 1] = jnp.sum(folded[r * tile:(r + 1) * tile].T, axis=0, keepdims=True)
        block = acts.at[i, tp]
        for h, dev, base in ((0, x_right, 1), (1, x_left, 3), (1, x_right, 1), (0, x_left, 3)):
            part = block.at[pl.ds(h * half_rows, half_rows)]
            begin(remote(part, part, ags_sem.at[i, base + h], agr_sem.at[i, base + h], dev))
        begin(remote(block, block, ags_sem.at[i, 0], agr_sem.at[i, 0], partner))
        for k in range(1, tpn):
            sq_ref = squares.at[i, tp]
            begin(remote(sq_ref, sq_ref, sqs_sem.at[i, k], sqr_sem.at[i, k], {"tp": lax.rem(tp + k, tpn)}))

    def ag_part(i, side, h, other_core=False):
        offset = (RING_X - 1, 1, 2)[side]
        c = 1 - core if other_core else core
        return acts.at[i, 2 * lax.rem(x + offset, RING_X) + c, pl.ds(h * half_rows, half_rows)]

    def ag_near(i):
        for side, h in ((0, 0), (1, 1), (0, 1), (1, 0)):
            part = ag_part(i, side, h)
            k = 1 + 2 * side + h
            remote(part, part, ags_sem.at[i, k], agr_sem.at[i, k], partner).wait_recv()
            if side == h:
                begin(remote(part, part, ags_sem.at[i, 5 + h], agr_sem.at[i, 5 + h], (x_right, x_left)[side]))
            begin(remote(part, part, ags_sem.at[i, 6 + k], agr_sem.at[i, 6 + k], partner))

    def ag_far(i):
        for h in range(2):
            part = ag_part(i, 2, h)
            k = 5 + h
            remote(part, part, ags_sem.at[i, k], agr_sem.at[i, k], partner).wait_recv()
            begin(remote(part, part, ags_sem.at[i, 6 + k], agr_sem.at[i, 6 + k], partner))

    def ag_end(i):
        for k in range(1, tpn):
            sq_ref = squares.at[i, lax.rem(tp + tpn - k, tpn)]
            remote(sq_ref, sq_ref, sqs_sem.at[i, k], sqr_sem.at[i, k], partner).wait_recv()
        total = squares[i, 0]
        for k in range(1, tpn):
            total = total + squares[i, k]
        factor = lax.rsqrt(total * (1.0 / features) + EPS)
        for r in range(3):
            factors[r * tile:(r + 1) * tile] = jnp.broadcast_to(factor[r:r + 1], (128, 128)).T
        block = acts.at[i, tp + 1 - 2 * core]
        remote(block, block, ags_sem.at[i, 0], agr_sem.at[i, 0], partner).wait_recv()
        for side in range(3):
            for h in range(2):
                part = ag_part(i, side, h, True)
                k = 7 + 2 * side + h
                remote(part, part, ags_sem.at[i, k], agr_sem.at[i, k], partner).wait_recv()

    def whole(i):
        return jnp.concatenate([acts[i, k] for k in range(tpn)], axis=1)

    def rs(i, block):
        def at(o, c):
            return 2 * lax.rem(x + o, RING_X) + c

        for k, o in enumerate(NEAR):
            pair_out[i, k] = block(at(o, 1 - core)).astype(BF16)
            begin(remote(pair_out.at[i, k], pair_in.at[i, k], rss_sem.at[i, k], rsr_sem.at[i, k], partner))

        def paired(k):
            product = block(at(NEAR[k], core))
            remote(pair_out.at[i, k], pair_in.at[i, k], rss_sem.at[i, k], rsr_sem.at[i, k], partner).wait_recv()
            return product + pair_in[i, k].astype(F32)

        low = pl.ds(0, half_rows)
        high = pl.ds(half_rows, half_rows)
        turn_out[i, 0] = paired(0).astype(BF16)
        begin(remote(turn_out.at[i, 0, low], mid_in.at[i, 0], rss_sem.at[i, 4], rsr_sem.at[i, 4], x_right))
        begin(remote(turn_out.at[i, 0, high], mid_in.at[i, 1], rss_sem.at[i, 5], rsr_sem.at[i, 5], x_left))
        right = paired(1)
        turn_out[i, 1, half_rows:] = right[half_rows:].astype(BF16)
        begin(remote(turn_out.at[i, 1, high], last_in.at[i, 0, high], rss_sem.at[i, 7], rsr_sem.at[i, 7], x_right))
        kept[0] = right[:half_rows]
        left = paired(2)
        turn_out[i, 2, :half_rows] = left[:half_rows].astype(BF16)
        begin(remote(turn_out.at[i, 2, low], last_in.at[i, 1, low], rss_sem.at[i, 8], rsr_sem.at[i, 8], x_left))
        kept[1] = left[half_rows:]
        own[...] = paired(3)
        remote(turn_out.at[i, 0, low], mid_in.at[i, 0], rss_sem.at[i, 4], rsr_sem.at[i, 4], x_right).wait_recv()
        turn_out[i, 1, :half_rows] = (kept[0] + mid_in[i, 0].astype(F32)).astype(BF16)
        begin(remote(turn_out.at[i, 1, low], last_in.at[i, 0, low], rss_sem.at[i, 6], rsr_sem.at[i, 6], x_right))
        remote(turn_out.at[i, 0, high], mid_in.at[i, 1], rss_sem.at[i, 5], rsr_sem.at[i, 5], x_left).wait_recv()
        turn_out[i, 2, half_rows:] = (kept[1] + mid_in[i, 1].astype(F32)).astype(BF16)
        begin(remote(turn_out.at[i, 2, high], last_in.at[i, 1, high], rss_sem.at[i, 9], rsr_sem.at[i, 9], x_left))
        for k, side, part in ((7, 0, high), (8, 1, low), (6, 0, low), (9, 1, high)):
            ref = last_in.at[i, side, part]
            remote(ref, ref, rss_sem.at[i, k], rsr_sem.at[i, k], x_right).wait_recv()
        return own[...] + last_in[i, 0].astype(F32) + last_in[i, 1].astype(F32)

    def gu(i, t):
        scaled = whole(i)
        for q in range(2):
            pre[q] = jnp.dot(scaled, wgu[q, t], preferred_element_type=F32)
        for s in range(third // 128):
            cols = slice(s * 128, (s + 1) * 128)
            gate = factors[...] * pre[0, :, cols]
            up = factors[...] * pre[1, :, cols]
            hidden[:, t * third + s * 128:t * third + (s + 1) * 128] = (gate / (1.0 + jnp.exp(-gate)) * up).astype(BF16)

    def down_block(j):
        parts = []
        for t in range(3):
            for h in range(2):
                parts.append(jnp.concatenate([wd[t, h, 2 * j], wd[t, h, 2 * j + 1]], axis=1))
        return jnp.dot(hidden[...], jnp.concatenate(parts, axis=0), preferred_element_type=F32)

    for copy in local[:early]:
        copy.wait()
    gu_ks, late_ks = (0, 1), (2, 3, 4, 5)
    for k in gu_ks:
        for direction in range(2):
            z_send(k, direction, 0)
    ag_begin(0, xin[...])
    for copy in local[early:]:
        copy.wait()
    for step in range(1, half_n + 1):
        if step == half_n:
            for k in late_ks:
                for direction in range(2):
                    z_send(k, direction, 0)
        z_step(gu_ks, (0,), step)
        if step == 1:
            ag_near(0)
        if step == 2:
            ag_far(0)
        if step == 3:
            ag_end(0)
    for step in range(1, half_n + 1):
        z_step(late_ks, (1, 2), step)
        if step == 1:
            y_wait_all(0)
        if 2 <= step < 5:
            gu(0, step - 2)
    y_wait_all(1)
    total = rs(0, down_block)
    first[...] = (xin[...].astype(F32) + 0.5 * total).astype(BF16)
    ag_begin(1, first[...])
    ag_near(1)
    ag_far(1)
    y_wait_all(2)
    ag_end(1)

    scaled = whole(1)
    weights = jnp.concatenate([wpg[t] for t in range(3)], axis=1)
    sums = jnp.dot(scaled, weights, preferred_element_type=F32)
    pool_pre = (factors[...] * sums[:, :128]).astype(BF16)
    for s in range(2):
        logit = factors[...] * sums[:, (1 + s) * 128:(2 + s) * 128]
        pre[0, :, s * 128:(s + 1) * 128] = 1.0 / (1.0 + jnp.exp(-logit))
    values = pool_pre.astype(F32)
    position = lax.broadcasted_iota(jnp.int32, (rows, 128), 0)
    window_id = lax.rem(tp, 4)
    running = values
    chosen = values
    for w in range(4):
        span = 1 << w
        lagged = jnp.where(position >= span, pltpu.roll(running, span, 0), 0.0)
        running = running + lagged
        counts = jnp.minimum(position + 1, 2 * span).astype(F32)
        chosen = jnp.where(window_id == w, running / counts, chosen)
    trail = (chosen - values).astype(BF16)
    mixed = jnp.dot(trail, mixw[0], preferred_element_type=F32)
    hidden[:, :128] = (mixed * pscale[...]).astype(BF16)

    def lift_block(j):
        both = jnp.concatenate([wo[2 * j], wo[2 * j + 1]], axis=1)
        return jnp.dot(hidden[:, :128], both, preferred_element_type=F32)

    total = rs(1, lift_block)
    second[...] = (first[...].astype(F32) + pre[0] * total).astype(BF16)
    ag_begin(2, second[...])
    ag_near(2)
    ag_far(2)
    ag_end(2)
    for t in range(3):
        gu(2, t)
    total = rs(2, down_block)
    out_ref[...] = (second[...].astype(F32) + 0.5 * total).astype(BF16)
    for copy in sent:
        copy.wait_send()


def per_device(n, tpn, *arrays):
    x, gate = arrays[0], arrays[2]
    rows, width = x.shape
    kdim, ff = gate.shape
    third = ff // 3
    vmem = pltpu.VMEM
    dma = pltpu.SemaphoreType.DMA
    half_n = n // 2
    any_spec = pl.BlockSpec(memory_space=pl.ANY)
    return pl.pallas_call(
        functools.partial(kernel, n),
        out_shape=jax.ShapeDtypeStruct((rows, width), BF16),
        in_specs=[any_spec] * len(arrays),
        out_specs=pl.BlockSpec(memory_space=pltpu.VMEM),
        scratch_shapes=[
            vmem((rows, width), BF16),
            vmem((3, 1, width), BF16),
            vmem((1, 128, 128), BF16),
            vmem((1, 128), F32),
            vmem((2, 3, n * kdim, third), BF16),
            vmem((3, 2, n, third // 2, 128), BF16),
            vmem((3, n * kdim, 128), BF16),
            vmem((n, 128, 128), BF16),
            vmem((3, tpn, rows, width), BF16),
            vmem((3, tpn, 8, 128), F32),
            vmem((rows, 128), F32),
            vmem((rows, ff), BF16),
            vmem((2, rows, third), F32),
            vmem((rows, width), BF16),
            vmem((rows, width), BF16),
            vmem((3, 4, rows, width), BF16),
            vmem((3, 4, rows, width), BF16),
            vmem((3, 3, rows, width), BF16),
            vmem((3, 2, rows // 2, width), BF16),
            vmem((3, 2, rows, width), BF16),
            vmem((2, rows // 2, width), F32),
            vmem((rows, width), F32),
            dma((24,)),
            dma((6, 2, half_n)),
            dma((6, 2, half_n)),
            dma((3, n)),
            dma((3, n)),
            dma((3, 13)),
            dma((3, 13)),
            dma((3, tpn)),
            dma((3, tpn)),
            dma((3, 10)),
            dma((3, 10)),
        ],
        compiler_params=pltpu.CompilerParams(
            collective_id=0, has_side_effects=True, vmem_limit_bytes=60 * 1024 * 1024
        ),
    )(*arrays)


def solution(mesh):
    return jax.shard_map(
        functools.partial(per_device, mesh.shape["fs"], mesh.shape["tp"]),
        mesh=mesh,
        in_specs=(
            P(("grp", "fs"), "tp"),
            P(None, "tp"),
            P("fs", "tp"),
            P("fs", "tp"),
            P("tp", "fs"),
            P(None, "tp"),
            P("fs", "tp"),
            P("fs", "tp"),
            P("tp", None, None),
            P(None, "tp"),
            P("tp", "fs"),
            P(None, "tp"),
        ),
        out_specs=P(("grp", "fs"), "tp"),
        check_vma=False,
    )
```

time: 388 us -> 180 us (0.46)
  Pallas kernels: 0 us -> 178 us
  waiting for transfers between devices: 166 us -> 0 us
  blocking collectives: 119 us -> 0 us
  starting transfers between devices: 26 us -> 0 us
  matrix products: 25.2 us -> 0 us
  local copies, waits for them, and re-layouts: 20.2 us -> 1.62 us
  other arithmetic: 17.6 us -> 0 us
  between operations: 13.6 us -> 0.01 us
    pallas_call x0 -> x1, Pallas kernels: none -> 178 us  [per_device(): pl.pallas_call(functools.partial(kernel, n), out_shape=jax.ShapeDtypeStru...]
    all_gather x3 -> x0, waiting for transfers between devices: 123 us -> none  [the longest x1 71.1 us: per_device(): down_whole = lax.all_gather(ffn_down_w, 'fs', axis=1, tiled=True)]
    all_to_all x7 -> x0, blocking collectives: 119 us -> none  [the longest x5 64 us: from_everyone(): lax.all_to_all(jnp.broadcast_to(value[None], (length, *value.shape)), axi...]
    all_to_all x3 -> x0, waiting for transfers between devices: 41.9 us -> none  [the longest x2 22.1 us: from_everyone(): lax.all_to_all(jnp.broadcast_to(value[None], (length, *value.shape)), axi...]
    all_to_all x3 -> x0, starting transfers between devices: 25.8 us -> none  [the longest x1 15.3 us: summed_on_arrival(): lax.all_to_all(tiles, axis, split_axis=0, concat_axis=0, tiled=True)]
    dot_general x7 -> x0, matrix products: 25.2 us -> none  [the longest x2 12.9 us: feed_forward(): return jnp.dot(hidden, down_whole, preferred_element_type=jnp.float32)]
    convert_element_type x13 -> x0, other arithmetic: 11.4 us -> none  [the longest x3 5.81 us: norm_rows(): widened = gathered.astype(jnp.float32)]
    convert_element_type x3 -> x0, local copies, waits for them, and re-layouts: 9.46 us -> none  [norm_rows(): widened = gathered.astype(jnp.float32)]
  transfers between devices with their start and end apart: 6 -> 0, of which waited for: 6 -> 0; matrix products, arithmetic and copies ran while one was open for 7% -> 0% of each run, Pallas kernels for 0% -> 0%
where the time goes in v1:
time: 180 us
  Pallas kernels  178 us (99%)
    pallas_call x1, Pallas kernels, per_device(): pl.pallas_call(functools.partial(kernel, n), out_shape=jax.ShapeDtypeStru...  178 us

profile of v1, /device:TPU:33, one launch (start us, length us, event | category | flops | bytes accessed | tf_op | source)
XLA Modules:
  0.0 180.1 jit_solution(7335762889291101299)
XLA Ops:
  0.0 178.5 %shard_map.118 = bf16[384,256]{1,0:T(8,128)(2,1)} custom-call(bf16[384,256]{1,0:T(8,128)(2,1)} %x_hbm.1, bf16[1,256]{1,0:T(2,128)(2,1)} %g1_hbm.1, bf16[128,768]{1,0:T(8,128)(2,1)} %gate_hbm.1, bf16[128,768]{1,0:T(8,128)(2,1)} %up_hbm.1, bf16[768,128]{1,0:T(8,128)(2,1)} %down_hbm.1, bf16[1,256]{1,0:T(2,128)(2,1)} %gm_hbm.1, bf16[128,128]{1,0:T(8,128)(2,1)} %pin_hbm.1, ...), custom_call_target="tpu_custom_call" | custom-call | tf_op jit(solution)/shard_map/pallas_call | solution.py:369
  178.5 1.6 copy.14

commit v2 on v1

--- a/solution.py
+++ b/solution.py
@@ -13,6 +13,7 @@
 EPS = 1e-06
 RING_X = 4
 NEAR = (2, 1, 3, 0)
+BATCH = (((1, -1), (2, -2)), ((3, -3), (4, -4)), ((5, -5), (6, -6)), ((7, -7), (0, 8)))
 
 
 def remote(src, dst, send, recv, device):
@@ -28,10 +29,11 @@
     xin, gains, mixw, pscale,
     wgu, wd, wpg, wo,
     acts, squares, factors, hidden, pre, first, second,
+    part, gp_out, gp_in, gt_out, gm_in, gl_in, fall, first_all, scaled_all, sq_sum,
     pair_out, pair_in, turn_out, mid_in, last_in, kept, own,
     in_sem,
     zs_sem, zr_sem, ys_sem, yr_sem,
-    ags_sem, agr_sem, sqs_sem, sqr_sem, rss_sem, rsr_sem,
+    ags_sem, agr_sem, sqs_sem, sqr_sem, rss_sem, rsr_sem, gs_sem, gr_sem,
 ):
     rows, width = x_hbm.shape
     half_rows = rows // 2
@@ -78,7 +80,7 @@
             fetch(ref.at[:, pl.ds(t * third, third)], wgu.at[q, t, own_rows])
     fetch(x_hbm, xin)
     for k, ref in enumerate((g1_hbm, gm_hbm, g2_hbm)):
-        fetch(ref, gains.at[k])
+        fetch(ref, gains.at[tp, k])
     early = len(local)
     for t in range(3):
         for h in range(2):
@@ -152,11 +154,14 @@
         region = y_kinds[kind](mine, shard(d))
         begin(remote(region, region, ys_sem.at[kind, d % n], yr_sem.at[kind, d % n], y_dev))
 
+    def y_wait(kind, d):
+        region = y_kinds[kind](other, shard(d))
+        remote(region, region, ys_sem.at[kind, d % n], yr_sem.at[kind, d % n], y_dev).wait_recv()
+
     def y_wait_all(kind):
         for step in range(1, half_n + 1):
             for d in (-step, step) if step < half_n else (step,):
-                region = y_kinds[kind](other, shard(d))
-                remote(region, region, ys_sem.at[kind, d % n], yr_sem.at[kind, d % n], y_dev).wait_recv()
+                y_wait(kind, d)
 
     def z_step(ks, kinds, step):
         for k in ks:
@@ -168,20 +173,23 @@
                 y_send(kind, d)
 
     def ag_begin(i, values):
-        wide = values.astype(F32)
-        acts[i, tp] = (wide * gains[i].astype(F32)).astype(BF16)
-        sq = wide * wide
-        folded = sq[:, :128] + sq[:, 128:]
-        squares[i, tp] = jnp.zeros((8, 128), F32)
-        for r in range(3):
-            squares[i, tp, r:r + 1] = jnp.sum(folded[r * tile:(r + 1) * tile].T, axis=0, keepdims=True)
+        if i == 0:
+            acts[i, tp] = values
+        else:
+            wide = values.astype(F32)
+            acts[i, tp] = (wide * gains[tp, i].astype(F32)).astype(BF16)
+            sq = wide * wide
+            folded = sq[:, :128] + sq[:, 128:]
+            squares[tp] = jnp.zeros((8, 128), F32)
+            for r in range(3):
+                squares[tp, r:r + 1] = jnp.sum(folded[r * tile:(r + 1) * tile].T, axis=0, keepdims=True)
         block = acts.at[i, tp]
         for h, dev, base in ((0, x_right, 1), (1, x_left, 3), (1, x_right, 1), (0, x_left, 3)):
             part = block.at[pl.ds(h * half_rows, half_rows)]
             begin(remote(part, part, ags_sem.at[i, base + h], agr_sem.at[i, base + h], dev))
         begin(remote(block, block, ags_sem.at[i, 0], agr_sem.at[i, 0], partner))
         for k in range(1, tpn):
-            sq_ref = squares.at[i, tp]
+            sq_ref = gains.at[tp] if i == 0 else squares.at[tp]
             begin(remote(sq_ref, sq_ref, sqs_sem.at[i, k], sqr_sem.at[i, k], {"tp": lax.rem(tp + k, tpn)}))
 
     def ag_part(i, side, h, other_core=False):
@@ -207,14 +215,15 @@
 
     def ag_end(i):
         for k in range(1, tpn):
-            sq_ref = squares.at[i, lax.rem(tp + tpn - k, tpn)]
+            sq_ref = (gains if i == 0 else squares).at[lax.rem(tp + tpn - k, tpn)]
             remote(sq_ref, sq_ref, sqs_sem.at[i, k], sqr_sem.at[i, k], partner).wait_recv()
-        total = squares[i, 0]
-        for k in range(1, tpn):
-            total = total + squares[i, k]
-        factor = lax.rsqrt(total * (1.0 / features) + EPS)
-        for r in range(3):
-            factors[r * tile:(r + 1) * tile] = jnp.broadcast_to(factor[r:r + 1], (128, 128)).T
+        if i > 0:
+            total = squares[0]
+            for k in range(1, tpn):
+                total = total + squares[k]
+            factor = lax.rsqrt(total * (1.0 / features) + EPS)
+            for r in range(3):
+                factors[r * tile:(r + 1) * tile] = jnp.broadcast_to(factor[r:r + 1], (128, 128)).T
         block = acts.at[i, tp + 1 - 2 * core]
         remote(block, block, ags_sem.at[i, 0], agr_sem.at[i, 0], partner).wait_recv()
         for side in range(3):
@@ -225,6 +234,118 @@
 
     def whole(i):
         return jnp.concatenate([acts[i, k] for k in range(tpn)], axis=1)
+
+    def factors_from_sum():
+        total = jnp.sum(sq_sum[...], axis=1, keepdims=True)
+        factors[...] = jnp.broadcast_to(lax.rsqrt(total * (1.0 / features) + EPS), (rows, 128))
+
+    def scale_input(k):
+        wide = acts[0, k].astype(F32)
+        acts[1, k] = (wide * gains[k, 0].astype(F32)).astype(BF16)
+        sq = wide * wide
+        both = sq[:, :128] + sq[:, 128:]
+        sq_sum[...] = both if k == 0 else sq_sum[...] + both
+
+    chunk = rows // tpn
+
+    def rows_at(o, c):
+        return pl.ds(pl.multiple_of((2 * lax.rem(x + o, RING_X) + c) * chunk, 16), chunk)
+
+    def g_remote(g, src, dst, k, dev):
+        return remote(src, dst, gs_sem.at[g, k], gr_sem.at[g, k], dev)
+
+    def g_wait(g, ref, k):
+        g_remote(g, ref, ref, k, partner).wait_recv()
+
+    def paired_sum(g, k, h):
+        return part[g, h, rows_at(NEAR[k], core)] + gp_in[g, k, h].astype(F32)
+
+    x_dev = (x_right, x_left)
+
+    def g_multiply(g):
+        for h in range(2):
+            for d in BATCH[g][h]:
+                if d != 0:
+                    y_wait(1, d)
+        for h in range(2):
+            d0, d1 = BATCH[g][h]
+            parts = []
+            for t in range(3):
+                for q in range(2):
+                    parts.append(jnp.concatenate([wd[t, q, shard(d0)], wd[t, q, shard(d1)]], axis=1))
+            part[g, h] = jnp.dot(hidden[...], jnp.concatenate(parts, axis=0), preferred_element_type=F32)
+        for k, o in enumerate(NEAR):
+            for h in range(2):
+                gp_out[g, k, h] = part[g, h, rows_at(o, 1 - core)].astype(BF16)
+        begin(g_remote(g, gp_out.at[g], gp_in.at[g], 0, partner))
+
+    def g_pair(g):
+        g_wait(g, gp_in.at[g], 0)
+        for h in range(2):
+            gt_out[g, 0, h] = paired_sum(g, 0, h).astype(BF16)
+            begin(g_remote(g, gt_out.at[g, 0, h], gm_in.at[g, h], 1 + h, x_dev[h]))
+        for side in range(2):
+            gt_out[g, 1 + side, 1 - side] = paired_sum(g, 1 + side, 1 - side).astype(BF16)
+            begin(g_remote(
+                g, gt_out.at[g, 1 + side, 1 - side], gl_in.at[g, side, 1 - side], 3 + 2 * side + 1 - side, x_dev[side]
+            ))
+
+    def g_turn(g):
+        for side in range(2):
+            g_wait(g, gm_in.at[g, side], 1 + side)
+            gt_out[g, 1 + side, side] = (paired_sum(g, 1 + side, side) + gm_in[g, side].astype(F32)).astype(BF16)
+            begin(g_remote(g, gt_out.at[g, 1 + side, side], gl_in.at[g, side, side], 3 + 3 * side, x_dev[side]))
+
+    def g_first(g):
+        for side in range(2):
+            for h in range(2):
+                g_wait(g, gl_in.at[g, side, h], 3 + 2 * side + h)
+        for h in range(2):
+            total = paired_sum(g, 3, h) + gl_in[g, 0, h].astype(F32) + gl_in[g, 1, h].astype(F32)
+            for e in range(2):
+                b = shard(BATCH[g][h][e])
+                both = acts[0, b // 2, pl.ds(pl.multiple_of(tp * chunk, 16), chunk)].astype(F32)
+                base = jnp.where(b % 2 == 1, both[:, 128:], both[:, :128])
+                cols = slice(e * 128, (e + 1) * 128)
+                fall[g, tp, h, :, cols] = (base + 0.5 * total[:, cols]).astype(BF16)
+        block = fall.at[g, tp]
+        begin(g_remote(g, block, block, 8, x_right))
+        begin(g_remote(g, block, block, 9, x_left))
+        begin(g_remote(g, block, block, 7, partner))
+
+    def fall_of(g, o, c):
+        return fall.at[g, 2 * lax.rem(x + o, RING_X) + c]
+
+    def g_near(g):
+        for side in range(2):
+            block = fall_of(g, (RING_X - 1, 1)[side], core)
+            g_wait(g, block, 8 + side)
+            begin(g_remote(g, block.at[side], block.at[side], 10 + side, x_dev[side]))
+            begin(g_remote(g, block, block, 12 + side, partner))
+
+    def g_far(g):
+        block = fall_of(g, 2, core)
+        for h in range(2):
+            g_wait(g, block.at[h], 10 + h)
+            begin(g_remote(g, block.at[h], block.at[h], 14 + h, partner))
+
+    def g_end(g):
+        g_wait(g, fall_of(g, 0, 1 - core), 7)
+        g_wait(g, fall_of(g, RING_X - 1, 1 - core), 12)
+        g_wait(g, fall_of(g, 1, 1 - core), 13)
+        for h in range(2):
+            g_wait(g, fall_of(g, 2, 1 - core).at[h], 14 + h)
+        for h in range(2):
+            for e in range(2):
+                b = shard(BATCH[g][h][e])
+                value = jnp.concatenate([fall[g, k, h, :, e * 128:(e + 1) * 128] for k in range(tpn)], axis=0)
+                first_all[b] = value
+                wide = value.astype(F32)
+                gain = gains[b // 2, 1].astype(F32)
+                gain = jnp.where(b % 2 == 1, gain[:, 128:], gain[:, :128])
+                scaled_all[b] = (wide * gain).astype(BF16)
+                sq = wide * wide
+                sq_sum[...] = sq if g == h == e == 0 else sq_sum[...] + sq
 
     def rs(i, block):
         def at(o, c):
@@ -290,11 +411,10 @@
     ag_begin(0, xin[...])
     for copy in local[early:]:
         copy.wait()
+    for k in late_ks:
+        for direction in range(2):
+            z_send(k, direction, 0)
     for step in range(1, half_n + 1):
-        if step == half_n:
-            for k in late_ks:
-                for direction in range(2):
-                    z_send(k, direction, 0)
         z_step(gu_ks, (0,), step)
         if step == 1:
             ag_near(0)
@@ -302,22 +422,29 @@
             ag_far(0)
         if step == 3:
             ag_end(0)
-    for step in range(1, half_n + 1):
-        z_step(late_ks, (1, 2), step)
-        if step == 1:
+        if 4 <= step < 8:
+            scale_input(2 * step - 8)
+            scale_input(2 * step - 7)
+    factors_from_sum()
+    stages = (g_multiply, g_pair, g_turn, g_first, g_near, g_far, g_end)
+    for slot in range(1, 2 * half_n + 1):
+        if slot <= half_n:
+            z_step((2, 3), (1,), slot)
+        else:
+            z_step((4, 5), (2,), slot - half_n)
+        if slot == 2:
             y_wait_all(0)
-        if 2 <= step < 5:
-            gu(0, step - 2)
-    y_wait_all(1)
-    total = rs(0, down_block)
-    first[...] = (xin[...].astype(F32) + 0.5 * total).astype(BF16)
-    ag_begin(1, first[...])
-    ag_near(1)
-    ag_far(1)
+        if 2 <= slot < 5:
+            gu(1, slot - 2)
+        for k, stage in reversed(tuple(enumerate(stages))):
+            g = (slot - 4 - k) // 2
+            if (slot - 4 - k) % 2 == 0 and 0 <= g < len(BATCH):
+                stage(g)
     y_wait_all(2)
-    ag_end(1)
-
-    scaled = whole(1)
+    factors_from_sum()
+    first[...] = jnp.concatenate([first_all[2 * tp], first_all[2 * tp + 1]], axis=1)
+
+    scaled = jnp.concatenate([scaled_all[b] for b in range(n)], axis=1)
     weights = jnp.concatenate([wpg[t] for t in range(3)], axis=1)
     sums = jnp.dot(scaled, weights, preferred_element_type=F32)
     pool_pre = (factors[...] * sums[:, :128]).astype(BF16)
@@ -362,6 +489,7 @@
     rows, width = x.shape
     kdim, ff = gate.shape
     third = ff // 3
+    chunk = rows // tpn
     vmem = pltpu.VMEM
     dma = pltpu.SemaphoreType.DMA
     half_n = n // 2
@@ -373,7 +501,7 @@
         out_specs=pl.BlockSpec(memory_space=pltpu.VMEM),
         scratch_shapes=[
             vmem((rows, width), BF16),
-            vmem((3, 1, width), BF16),
+            vmem((tpn, 3, 1, width), BF16),
             vmem((1, 128, 128), BF16),
             vmem((1, 128), F32),
             vmem((2, 3, n * kdim, third), BF16),
@@ -381,12 +509,22 @@
             vmem((3, n * kdim, 128), BF16),
             vmem((n, 128, 128), BF16),
             vmem((3, tpn, rows, width), BF16),
-            vmem((3, tpn, 8, 128), F32),
+            vmem((tpn, 8, 128), F32),
             vmem((rows, 128), F32),
             vmem((rows, ff), BF16),
             vmem((2, rows, third), F32),
             vmem((rows, width), BF16),
             vmem((rows, width), BF16),
+            vmem((4, 2, rows, width), F32),
+            vmem((4, 4, 2, chunk, width), BF16),
+            vmem((4, 4, 2, chunk, width), BF16),
+            vmem((4, 3, 2, chunk, width), BF16),
+            vmem((4, 2, chunk, width), BF16),
+            vmem((4, 2, 2, chunk, width), BF16),
+            vmem((4, tpn, 2, chunk, width), BF16),
+            vmem((n, rows, 128), BF16),
+            vmem((n, rows, 128), BF16),
+            vmem((rows, 128), F32),
             vmem((3, 4, rows, width), BF16),
             vmem((3, 4, rows, width), BF16),
             vmem((3, 3, rows, width), BF16),
@@ -405,6 +543,8 @@
             dma((3, tpn)),
             dma((3, 10)),
             dma((3, 10)),
+            dma((4, 16)),
+            dma((4, 16)),
         ],
         compiler_params=pltpu.CompilerParams(
             collective_id=0, has_side_effects=True, vmem_limit_bytes=60 * 1024 * 1024

time: 180 us -> 182 us (1.011)
  Pallas kernels: 178 us -> 180 us
where the time goes in v2:
time: 182 us
  Pallas kernels  180 us (99%)
    pallas_call x1, Pallas kernels, per_device(): pl.pallas_call(functools.partial(kernel, n), out_shape=jax.ShapeDtypeStru...  180 us

profile of v2, /device:TPU:33, one launch (start us, length us, event | category | flops | bytes accessed | tf_op | source)
XLA Modules:
  0.0 181.8 jit_solution(3072261335232115661)
XLA Ops:
  0.0 180.2 %shard_map.118 = bf16[384,256]{1,0:T(8,128)(2,1)} custom-call(bf16[384,256]{1,0:T(8,128)(2,1)} %x_hbm.1, bf16[1,256]{1,0:T(2,128)(2,1)} %g1_hbm.1, bf16[128,768]{1,0:T(8,128)(2,1)} %gate_hbm.1, bf16[128,768]{1,0:T(8,128)(2,1)} %up_hbm.1, bf16[768,128]{1,0:T(8,128)(2,1)} %down_hbm.1, bf16[1,256]{1,0:T(2,128)(2,1)} %gm_hbm.1, bf16[128,128]{1,0:T(8,128)(2,1)} %pin_hbm.1, ...), custom_call_target="tpu_custom_call" | custom-call | tf_op jit(solution)/shard_map/pallas_call | solution.py:497
  180.2 1.6 copy.14

commit v3 on v2

--- a/solution.py
+++ b/solution.py
@@ -29,7 +29,7 @@
     xin, gains, mixw, pscale,
     wgu, wd, wpg, wo,
     acts, squares, factors, hidden, pre, first, second,
-    part, gp_out, gp_in, gt_out, gm_in, gl_in, fall, first_all, scaled_all, sq_sum,
+    mixed_in, part, gp_out, gp_in, gt_out, gm_in, gl_in, fall, first_all, scaled_all, sq_sum,
     pair_out, pair_in, turn_out, mid_in, last_in, kept, own,
     in_sem,
     zs_sem, zr_sem, ys_sem, yr_sem,
@@ -111,11 +111,8 @@
     def z_up(s):
         return wgu.at[1, pl.ds(parity, 2), rows_of(s)]
 
-    def z_down0(s):
-        return wd.at[pl.ds(parity, 2), 0, s]
-
-    def z_down1(s):
-        return wd.at[pl.ds(parity, 2), 1, s]
+    def z_down(t, q):
+        return lambda s: wd.at[parity + t, q, s]
 
     def z_pool(s):
         return wpg.at[pl.ds(parity, 2), rows_of(s)]
@@ -124,8 +121,8 @@
         return wo.at[s]
 
     half_n = n // 2
-    chains = (z_gate, z_up, z_down0, z_down1, z_pool, z_lift)
-    hops = ((half_n, half_n - 1), (half_n - 1, half_n)) * 3
+    chains = (z_gate, z_up, z_pool, z_lift, z_down(0, 0), z_down(1, 1), z_down(1, 0), z_down(0, 1))
+    hops = ((half_n, half_n - 1), (half_n - 1, half_n)) * 4
 
     def y_gu(slot, s):
         return wgu.at[:, slot, rows_of(s)]
@@ -346,6 +343,13 @@
                 scaled_all[b] = (wide * gain).astype(BF16)
                 sq = wide * wide
                 sq_sum[...] = sq if g == h == e == 0 else sq_sum[...] + sq
+        blocks = [shard(d) for pair in BATCH[g] for d in pair]
+        left = jnp.concatenate([scaled_all[b] for b in blocks], axis=1)
+        right = jnp.concatenate(
+            [jnp.concatenate([wpg[t, rows_of(b)] for t in range(3)], axis=1) for b in blocks], axis=0
+        )
+        product = jnp.dot(left, right, preferred_element_type=F32)
+        mixed_in[...] = product if g == 0 else mixed_in[...] + product
 
     def rs(i, block):
         def at(o, c):
@@ -404,18 +408,22 @@
 
     for copy in local[:early]:
         copy.wait()
-    gu_ks, late_ks = (0, 1), (2, 3, 4, 5)
-    for k in gu_ks:
+    head, tail = (0, 1, 2, 3), (4, 5, 6, 7)
+    for k in (0, 1):
         for direction in range(2):
             z_send(k, direction, 0)
     ag_begin(0, xin[...])
     for copy in local[early:]:
         copy.wait()
-    for k in late_ks:
+    for k in (2, 3):
         for direction in range(2):
             z_send(k, direction, 0)
     for step in range(1, half_n + 1):
-        z_step(gu_ks, (0,), step)
+        if step == half_n:
+            for k in tail:
+                for direction in range(2):
+                    z_send(k, direction, 0)
+        z_step(head, (0, 2), step)
         if step == 1:
             ag_near(0)
         if step == 2:
@@ -427,29 +435,27 @@
             scale_input(2 * step - 7)
     factors_from_sum()
     stages = (g_multiply, g_pair, g_turn, g_first, g_near, g_far, g_end)
-    for slot in range(1, 2 * half_n + 1):
+    for slot in range(1, 2 * half_n):
         if slot <= half_n:
-            z_step((2, 3), (1,), slot)
-        else:
-            z_step((4, 5), (2,), slot - half_n)
+            z_step(tail, (1,), slot)
         if slot == 2:
             y_wait_all(0)
-        if 2 <= slot < 5:
-            gu(1, slot - 2)
+            gu(1, 0)
+            gu(1, 1)
+        if slot == 3:
+            gu(1, 2)
+        if slot == half_n:
+            y_wait_all(2)
         for k, stage in reversed(tuple(enumerate(stages))):
-            g = (slot - 4 - k) // 2
-            if (slot - 4 - k) % 2 == 0 and 0 <= g < len(BATCH):
+            g = (slot - 3 - k) // 2
+            if (slot - 3 - k) % 2 == 0 and 0 <= g < len(BATCH):
                 stage(g)
-    y_wait_all(2)
     factors_from_sum()
     first[...] = jnp.concatenate([first_all[2 * tp], first_all[2 * tp + 1]], axis=1)
 
-    scaled = jnp.concatenate([scaled_all[b] for b in range(n)], axis=1)
-    weights = jnp.concatenate([wpg[t] for t in range(3)], axis=1)
-    sums = jnp.dot(scaled, weights, preferred_element_type=F32)
-    pool_pre = (factors[...] * sums[:, :128]).astype(BF16)
+    pool_pre = (factors[...] * mixed_in[:, :128]).astype(BF16)
     for s in range(2):
-        logit = factors[...] * sums[:, (1 + s) * 128:(2 + s) * 128]
+        logit = factors[...] * mixed_in[:, (1 + s) * 128:(2 + s) * 128]
         pre[0, :, s * 128:(s + 1) * 128] = 1.0 / (1.0 + jnp.exp(-logit))
     values = pool_pre.astype(F32)
     position = lax.broadcasted_iota(jnp.int32, (rows, 128), 0)
@@ -515,6 +521,7 @@
             vmem((2, rows, third), F32),
             vmem((rows, width), BF16),
             vmem((rows, width), BF16),
+            vmem((rows, 384), F32),
             vmem((4, 2, rows, width), F32),
             vmem((4, 4, 2, chunk, width), BF16),
             vmem((4, 4, 2, chunk, width), BF16),
@@ -533,8 +540,8 @@
             vmem((2, rows // 2, width), F32),
             vmem((rows, width), F32),
             dma((24,)),
-            dma((6, 2, half_n)),
-            dma((6, 2, half_n)),
+            dma((8, 2, half_n)),
+            dma((8, 2, half_n)),
             dma((3, n)),
             dma((3, n)),
             dma((3, 13)),

time: 182 us -> 189 us (1.038)
  Pallas kernels: 180 us -> 187 us
    pallas_call x1, Pallas kernels: 180 us -> 187 us  [per_device(): pl.pallas_call(functools.partial(kernel, n), out_shape=jax.ShapeDtypeStru...]
where the time goes in v3:
time: 189 us
  Pallas kernels  187 us (99%)
    pallas_call x1, Pallas kernels, per_device(): pl.pallas_call(functools.partial(kernel, n), out_shape=jax.ShapeDtypeStru...  187 us

profile of v3, /device:TPU:33, one launch (start us, length us, event | category | flops | bytes accessed | tf_op | source)
XLA Modules:
  0.0 188.6 jit_solution(6980048762628645469)
XLA Ops:
  0.0 187.0 %shard_map.118 = bf16[384,256]{1,0:T(8,128)(2,1)} custom-call(bf16[384,256]{1,0:T(8,128)(2,1)} %x_hbm.1, bf16[1,256]{1,0:T(2,128)(2,1)} %g1_hbm.1, bf16[128,768]{1,0:T(8,128)(2,1)} %gate_hbm.1, bf16[128,768]{1,0:T(8,128)(2,1)} %up_hbm.1, bf16[768,128]{1,0:T(8,128)(2,1)} %down_hbm.1, bf16[1,256]{1,0:T(2,128)(2,1)} %gm_hbm.1, bf16[128,128]{1,0:T(8,128)(2,1)} %pin_hbm.1, ...), custom_call_target="tpu_custom_call" | custom-call | tf_op jit(solution)/shard_map/pallas_call | solution.py:503
  187.0 1.6 copy.14

commit v4 on v1

v4 whole, which is shorter than its diff:
```python
import functools

import jax
import jax.numpy as jnp
from jax import lax
from jax.experimental import pallas as pl
from jax.experimental.pallas import tpu as pltpu
from jax.sharding import PartitionSpec as P

F32 = jnp.float32
BF16 = jnp.bfloat16
MESH = pl.DeviceIdType.MESH
EPS = 1e-06
RING_X = 4
NEAR = (2, 1, 3, 0)


def remote(src, dst, send, recv, device):
    return pltpu.make_async_remote_copy(
        src_ref=src, dst_ref=dst, send_sem=send, recv_sem=recv, device_id=device, device_id_type=MESH
    )


def kernel(
    n,
    x_hbm, g1_hbm, gate_hbm, up_hbm, down_hbm, gm_hbm, pin_hbm, mg_hbm, mix_hbm, ps_hbm, mo_hbm, g2_hbm,
    out_ref,
    xin, gains, mixw, pscale,
    wgu, wd, wpg, wo,
    acts, squares, factors, hidden, pre, opened, pooling, first, second,
    pair_out, pair_in, turn_out, mid_in, last_in, kept, own,
    in_sem,
    zs_sem, zr_sem, ys_sem, yr_sem,
    ags_sem, agr_sem, sqs_sem, sqr_sem, rss_sem, rsr_sem,
):
    rows, width = x_hbm.shape
    part_rows = rows // 2
    half_rows = part_rows // 2
    kdim = gate_hbm.shape[0]
    third = gate_hbm.shape[1] // 3
    half_third = third // 2
    tpn = lax.axis_size("tp")
    features = tpn * width

    grp = lax.axis_index("grp")
    fs = lax.axis_index("fs")
    tp = lax.axis_index("tp")
    x = tp // 2
    core = tp % 2
    parity = grp % 2
    mine = 2 * parity
    other = 2 - mine

    z_right = {"fs": lax.rem(fs + 1, n)}
    z_left = {"fs": lax.rem(fs + n - 1, n)}
    z_dev = (z_right, z_left)
    y_dev = {"grp": grp + 1 - 2 * parity}
    partner = {"tp": tp + 1 - 2 * core}
    x_right = {"tp": lax.rem(tp + 2, tpn)}
    x_left = {"tp": lax.rem(tp + tpn - 2, tpn)}

    sent = []

    def begin(copy):
        copy.start()
        sent.append(copy)

    own_rows = pl.ds(pl.multiple_of(fs * kdim, kdim), kdim)
    local = []

    def fetch(src, dst):
        copy = pltpu.make_async_copy(src, dst, in_sem.at[len(local)])
        copy.start()
        local.append(copy)

    for q, ref in enumerate((gate_hbm, up_hbm)):
        for t in range(3):
            fetch(ref.at[:, pl.ds(t * third, third)], wgu.at[q, t, own_rows])
    fetch(x_hbm, xin)
    for k, ref in enumerate((g1_hbm, gm_hbm, g2_hbm)):
        fetch(ref, gains.at[k])
    early = len(local)
    for t in range(3):
        for h in range(2):
            fetch(down_hbm.at[pl.ds(t * third + h * half_third, half_third)], wd.at[t, h, fs])
    fetch(pin_hbm, wpg.at[0, own_rows])
    for t in range(2):
        fetch(mg_hbm.at[:, pl.ds(t * 128, 128)], wpg.at[1 + t, own_rows])
    fetch(mo_hbm, wo.at[fs])
    fetch(mix_hbm, mixw)
    fetch(ps_hbm, pscale)

    barrier = pltpu.get_barrier_semaphore()
    for dev in (z_right, z_left, y_dev):
        pl.semaphore_signal(barrier, inc=1, device_id=dev, device_id_type=MESH)
    for k in range(1, tpn):
        pl.semaphore_signal(barrier, inc=1, device_id={"tp": lax.rem(tp + k, tpn)}, device_id_type=MESH)
    pl.semaphore_wait(barrier, 3 + tpn - 1)

    def shard(d):
        return lax.rem(fs + n + d, n)

    def rows_of(s):
        return pl.ds(pl.multiple_of(s * kdim, kdim), kdim)

    def z_gu(q):
        return lambda s: wgu.at[q, pl.ds(parity, 2), rows_of(s)]

    def z_down(slot, q):
        return lambda s: wd.at[slot, q, s]

    def z_pool(t):
        return lambda s: wpg.at[t, rows_of(s)]

    half_n = n // 2
    gu_ks, down_ks, mix_ks = (0, 1), (2, 3, 4, 5), (6, 7, 8, 9)
    chains = (
        z_gu(0), z_gu(1), z_down(mine, 0), z_down(mine, 1), z_down(1, 0), z_down(1, 1),
        z_pool(0), z_pool(1), z_pool(2), lambda s: wo.at[s],
    )
    hops = ((half_n, half_n - 1), (half_n - 1, half_n)) * 5

    def y_gu(q):
        return lambda slot, s: wgu.at[q, slot, rows_of(s)]

    def y_down(slot, s):
        return wd.at[slot, :, s]

    y_kinds = (y_gu(0), y_gu(1), y_down)

    def z_send(k, direction, step):
        region = chains[k](shard(-step if direction == 0 else step))
        begin(remote(region, region, zs_sem.at[k, direction, step], zr_sem.at[k, direction, step], z_dev[direction]))

    def z_wait(k, direction, step):
        region = chains[k](shard(-step if direction == 0 else step))
        remote(
            region, region, zs_sem.at[k, direction, step - 1], zr_sem.at[k, direction, step - 1], z_dev[direction]
        ).wait_recv()
        if step < hops[k][direction]:
            z_send(k, direction, step)

    def y_send(kind, d):
        region = y_kinds[kind](mine, shard(d))
        begin(remote(region, region, ys_sem.at[kind, d % n], yr_sem.at[kind, d % n], y_dev))

    def y_wait_all(kind):
        for step in range(1, half_n + 1):
            for d in (-step, step) if step < half_n else (step,):
                region = y_kinds[kind](other, shard(d))
                remote(region, region, ys_sem.at[kind, d % n], yr_sem.at[kind, d % n], y_dev).wait_recv()

    def z_step(ks, step):
        for k in ks:
            for direction in range(2):
                if step <= hops[k][direction]:
                    z_wait(k, direction, step)
                    if k in gu_ks:
                        y_send(k, -step if direction == 0 and step < half_n else step)
            if k == down_ks[1]:
                for d in (-step, step) if step < half_n else (step,):
                    y_send(2, d)

    def ag_part(i, u, side, h, other_core=False):
        offset = (RING_X - 1, 1, 2)[side]
        c = 1 - core if other_core else core
        return acts.at[i, u, 2 * lax.rem(x + offset, RING_X) + c, pl.ds(h * half_rows, half_rows)]

    def ag(i, u, values):
        def move(ref, k, dev):
            return remote(ref, ref, ags_sem.at[i, u, k], agr_sem.at[i, u, k], dev)

        def move_sq(ref, k, dev):
            return remote(ref, ref, sqs_sem.at[i, u, k], sqr_sem.at[i, u, k], dev)

        wide = values.astype(F32)
        acts[i, u, tp] = (wide * gains[i].astype(F32)).astype(BF16)
        block = acts.at[i, u, tp]
        for h, dev, base in ((0, x_right, 1), (1, x_left, 3), (1, x_right, 1), (0, x_left, 3)):
            begin(move(block.at[pl.ds(h * half_rows, half_rows)], base + h, dev))
        begin(move(block, 0, partner))
        sq = wide * wide
        folded = sq[:, :128] + sq[:, 128:]
        squares[i, u, tp] = jnp.zeros((8, 128), F32)
        for r in range(2):
            start = r * (part_rows - 128)
            squares[i, u, tp, r:r + 1] = jnp.sum(folded[start:start + 128].T, axis=0, keepdims=True)
        for k in range(1, tpn):
            begin(move_sq(squares.at[i, u, tp], k, {"tp": lax.rem(tp + k, tpn)}))
        yield
        for side, h in ((0, 0), (1, 1), (0, 1), (1, 0)):
            part = ag_part(i, u, side, h)
            k = 1 + 2 * side + h
            move(part, k, partner).wait_recv()
            if side == h:
                begin(move(part, 5 + h, (x_right, x_left)[side]))
            begin(move(part, 6 + k, partner))
        yield
        for h in range(2):
            part = ag_part(i, u, 2, h)
            move(part, 5 + h, partner).wait_recv()
            begin(move(part, 11 + h, partner))
        yield
        for k in range(1, tpn):
            move_sq(squares.at[i, u, lax.rem(tp + tpn - k, tpn)], k, partner).wait_recv()
        total = squares[i, u, 0]
        for k in range(1, tpn):
            total = total + squares[i, u, k]
        factor = lax.rsqrt(total * (1.0 / features) + EPS)
        tall = [jnp.broadcast_to(factor[r:r + 1], (128, 128)).T for r in range(2)]
        factors[i, u, :128] = tall[0]
        factors[i, u, 128:] = tall[1][256 - part_rows:]
        move(acts.at[i, u, tp + 1 - 2 * core], 0, partner).wait_recv()
        for side in range(3):
            for h in range(2):
                move(ag_part(i, u, side, h, True), 7 + 2 * side + h, partner).wait_recv()

    def whole(i, u):
        return jnp.concatenate([acts[i, u, k] for k in range(tpn)], axis=1)

    def half(u):
        return slice(u * part_rows, (u + 1) * part_rows)

    def rs(i, u, block, finish):
        def at(o, c):
            return 2 * lax.rem(x + o, RING_X) + c

        def move(src, dst, k, dev):
            return remote(src, dst, rss_sem.at[i, u, k], rsr_sem.at[i, u, k], dev)

        out, turn, kept_u = pair_out.at[i, u], turn_out.at[i, u], kept.at[u]
        came, mid, last = pair_in.at[i, u], mid_in.at[i, u], last_in.at[i, u]
        for k, o in enumerate(NEAR):
            out[k] = block(at(o, 1 - core)).astype(BF16)
            begin(move(out.at[k], came.at[k], k, partner))
        yield

        def paired(k):
            product = block(at(NEAR[k], core))
            move(out.at[k], came.at[k], k, partner).wait_recv()
            return product + came[k].astype(F32)

        low = pl.ds(0, half_rows)
        high = pl.ds(half_rows, half_rows)
        turn[0] = paired(0).astype(BF16)
        begin(move(turn.at[0, low], mid.at[0], 4, x_right))
        begin(move(turn.at[0, high], mid.at[1], 5, x_left))
        right = paired(1)
        turn[1, half_rows:] = right[half_rows:].astype(BF16)
        begin(move(turn.at[1, high], last.at[0, high], 7, x_right))
        kept_u[0] = right[:half_rows]
        left = paired(2)
        turn[2, :half_rows] = left[:half_rows].astype(BF16)
        begin(move(turn.at[2, low], last.at[1, low], 8, x_left))
        kept_u[1] = left[half_rows:]
        own[u] = paired(3)
        yield
        move(mid.at[0], mid.at[0], 4, x_right).wait_recv()
        turn[1, :half_rows] = (kept_u[0] + mid[0].astype(F32)).astype(BF16)
        begin(move(turn.at[1, low], last.at[0, low], 6, x_right))
        move(mid.at[1], mid.at[1], 5, x_left).wait_recv()
        turn[2, half_rows:] = (kept_u[1] + mid[1].astype(F32)).astype(BF16)
        begin(move(turn.at[2, high], last.at[1, high], 9, x_left))
        yield
        for k, side, part in ((7, 0, high), (8, 1, low), (6, 0, low), (9, 1, high)):
            move(last.at[side, part], last.at[side, part], k, x_right).wait_recv()
        finish(own[u] + last[0].astype(F32) + last[1].astype(F32))

    def gu(i, u, t):
        scaled = whole(i, u)
        for q in range(2):
            pre[q] = jnp.dot(scaled, wgu[q, t], preferred_element_type=F32)
        for s in range(third // 128):
            cols = slice(s * 128, (s + 1) * 128)
            gate = factors[i, u] * pre[0, :, cols]
            up = factors[i, u] * pre[1, :, cols]
            hidden[half(u), t * third + s * 128:t * third + (s + 1) * 128] = (
                gate / (1.0 + jnp.exp(-gate)) * up
            ).astype(BF16)

    def down_block(u):
        def block(j):
            parts = []
            for t in range(3):
                for h in range(2):
                    parts.append(jnp.concatenate([wd[t, h, 2 * j], wd[t, h, 2 * j + 1]], axis=1))
            return jnp.dot(hidden[half(u)], jnp.concatenate(parts, axis=0), preferred_element_type=F32)

        return block

    def lift_block(u):
        def block(j):
            both = jnp.concatenate([wo[2 * j], wo[2 * j + 1]], axis=1)
            return jnp.dot(hidden[half(u), :128], both, preferred_element_type=F32)

        return block

    def set_first(u):
        def finish(total):
            first[half(u)] = (xin[half(u)].astype(F32) + 0.5 * total).astype(BF16)

        return finish

    def set_second(u):
        def finish(total):
            second[half(u)] = (first[half(u)].astype(F32) + opened[half(u)] * total).astype(BF16)

        return finish

    def set_out(u):
        def finish(total):
            out_ref[half(u)] = (second[half(u)].astype(F32) + 0.5 * total).astype(BF16)

        return finish

    def mix(u):
        weights = jnp.concatenate([wpg[t] for t in range(3)], axis=1)
        sums = jnp.dot(whole(1, u), weights, preferred_element_type=F32)
        scale = factors[1, u]
        for s in range(2):
            logit = scale * sums[:, (1 + s) * 128:(2 + s) * 128]
            opened[half(u), s * 128:(s + 1) * 128] = 1.0 / (1.0 + jnp.exp(-logit))
        pooling[16 + u * part_rows:16 + (u + 1) * part_rows] = (scale * sums[:, :128]).astype(BF16).astype(F32)
        if u == 0:
            pooling[:16] = jnp.zeros((16, 128), F32)
        size = part_rows + 16
        values = pooling[u * part_rows:u * part_rows + size]
        position = lax.broadcasted_iota(jnp.int32, (size, 128), 0) + (u * part_rows - 16)
        window_id = lax.rem(tp, 4)
        running = values
        chosen = values
        for w in range(4):
            span = 1 << w
            running = running + pltpu.roll(running, span, 0)
            counts = jnp.clip(position + 1, 1, 2 * span).astype(F32)
            chosen = jnp.where(window_id == w, running / counts, chosen)
        trail = (chosen - values)[16:].astype(BF16)
        mixed = jnp.dot(trail, mixw[0], preferred_element_type=F32)
        hidden[half(u), :128] = (mixed * pscale[...]).astype(BF16)

    def layer(u):
        yield from rs(0, u, down_block(u), set_first(u))
        yield from ag(1, u, first[half(u)])
        mix(u)
        yield from rs(1, u, lift_block(u), set_second(u))
        yield from ag(2, u, second[half(u)])
        for t in range(3):
            gu(2, u, t)
        yield from rs(2, u, down_block(u), set_out(u))

    def advance(steps):
        for step in steps:
            next(step, None)

    def send_own(ks):
        for k in ks:
            for direction in range(2):
                z_send(k, direction, 0)

    for copy in local[:early]:
        copy.wait()
    send_own(gu_ks)
    inputs = [ag(0, u, xin[half(u)]) for u in range(2)]
    advance(inputs)
    for copy in local[early:]:
        copy.wait()
    for step in range(1, half_n + 1):
        if step == half_n:
            send_own(down_ks)
        z_step(gu_ks, step)
        if step > 1:
            advance(inputs)
    todo = [(u, t) for u in range(2) for t in range(3)]
    for step in range(1, half_n + 1):
        if step == half_n - 1:
            send_own(mix_ks)
        z_step(down_ks, step)
        if step == 2:
            y_wait_all(0)
            y_wait_all(1)
        if step >= 2:
            for u, t in todo[:2 if step in (3, 4) else 1]:
                gu(0, u, t)
            todo = todo[2 if step in (3, 4) else 1:]
    mix_steps = list(range(1, half_n + 1))

    def mix_step():
        if mix_steps:
            z_step(mix_ks, mix_steps.pop(0))

    mix_step()
    y_wait_all(2)
    mix_step()
    halves = [layer(u) for u in range(2)]
    for turn_number in range(24):
        advance(halves)
        mix_step()
    for copy in sent:
        copy.wait_send()


def per_device(n, tpn, *arrays):
    x, gate = arrays[0], arrays[2]
    rows, width = x.shape
    kdim, ff = gate.shape
    third = ff // 3
    part = rows // 2
    vmem = pltpu.VMEM
    dma = pltpu.SemaphoreType.DMA
    half_n = n // 2
    any_spec = pl.BlockSpec(memory_space=pl.ANY)
    return pl.pallas_call(
        functools.partial(kernel, n),
        out_shape=jax.ShapeDtypeStruct((rows, width), BF16),
        in_specs=[any_spec] * len(arrays),
        out_specs=pl.BlockSpec(memory_space=pltpu.VMEM),
        scratch_shapes=[
            vmem((rows, width), BF16),
            vmem((3, 1, width), BF16),
            vmem((1, 128, 128), BF16),
            vmem((1, 128), F32),
            vmem((2, 3, n * kdim, third), BF16),
            vmem((3, 2, n, third // 2, 128), BF16),
            vmem((3, n * kdim, 128), BF16),
            vmem((n, 128, 128), BF16),
            vmem((3, 2, tpn, part, width), BF16),
            vmem((3, 2, tpn, 8, 128), F32),
            vmem((3, 2, part, 128), F32),
            vmem((rows, ff), BF16),
            vmem((2, part, third), F32),
            vmem((rows, width), F32),
            vmem((rows + 16, 128), F32),
            vmem((rows, width), BF16),
            vmem((rows, width), BF16),
            vmem((3, 2, 4, part, width), BF16),
            vmem((3, 2, 4, part, width), BF16),
            vmem((3, 2, 3, part, width), BF16),
            vmem((3, 2, 2, part // 2, width), BF16),
            vmem((3, 2, 2, part, width), BF16),
            vmem((2, 2, part // 2, width), F32),
            vmem((2, part, width), F32),
            dma((24,)),
            dma((10, 2, half_n)),
            dma((10, 2, half_n)),
            dma((3, n)),
            dma((3, n)),
            dma((3, 2, 13)),
            dma((3, 2, 13)),
            dma((3, 2, tpn)),
            dma((3, 2, tpn)),
            dma((3, 2, 10)),
            dma((3, 2, 10)),
        ],
        compiler_params=pltpu.CompilerParams(
            collective_id=0, has_side_effects=True, vmem_limit_bytes=60 * 1024 * 1024
        ),
    )(*arrays)


def solution(mesh):
    return jax.shard_map(
        functools.partial(per_device, mesh.shape["fs"], mesh.shape["tp"]),
        mesh=mesh,
        in_specs=(
            P(("grp", "fs"), "tp"),
            P(None, "tp"),
            P("fs", "tp"),
            P("fs", "tp"),
            P("tp", "fs"),
            P(None, "tp"),
            P("fs", "tp"),
            P("fs", "tp"),
            P("tp", None, None),
            P(None, "tp"),
            P("tp", "fs"),
            P(None, "tp"),
        ),
        out_specs=P(("grp", "fs"), "tp"),
        check_vma=False,
    )
```

time: 180 us -> 174 us (0.967)
  Pallas kernels: 178 us -> 171 us
    pallas_call x1, Pallas kernels: 178 us -> 171 us  [per_device(): pl.pallas_call(functools.partial(kernel, n), out_shape=jax.ShapeDtypeStru...]
where the time goes in v4:
time: 174 us; the launch traced here: 173 us
  Pallas kernels  171 us (98%)
    pallas_call x1, Pallas kernels, per_device(): pl.pallas_call(functools.partial(kernel, n), out_shape=jax.ShapeDtypeStru...  171 us

profile of v4, /device:TPU:33, one launch (start us, length us, event | category | flops | bytes accessed | tf_op | source)
XLA Modules:
  0.0 172.7 jit_solution(7253803539344039218)
XLA Ops:
  0.0 171.1 %shard_map.118 = bf16[384,256]{1,0:T(8,128)(2,1)} custom-call(bf16[384,256]{1,0:T(8,128)(2,1)} %x_hbm.1, bf16[1,256]{1,0:T(2,128)(2,1)} %g1_hbm.1, bf16[128,768]{1,0:T(8,128)(2,1)} %gate_hbm.1, bf16[128,768]{1,0:T(8,128)(2,1)} %up_hbm.1, bf16[768,128]{1,0:T(8,128)(2,1)} %down_hbm.1, bf16[1,256]{1,0:T(2,128)(2,1)} %gm_hbm.1, bf16[128,128]{1,0:T(8,128)(2,1)} %pin_hbm.1, ...), custom_call_target="tpu_custom_call" | custom-call | tf_op jit(solution)/shard_map/pallas_call | solution.py:412
  171.1 1.6 copy.14

commit v5 on v4

--- a/solution.py
+++ b/solution.py
@@ -27,7 +27,7 @@
     out_ref,
     xin, gains, mixw, pscale,
     wgu, wd, wpg, wo,
-    acts, squares, factors, hidden, pre, opened, pooling, first, second,
+    acts, squares, core_sums, factors, hidden, pre, opened, pooling, first, second,
     pair_out, pair_in, turn_out, mid_in, last_in, kept, own,
     in_sem,
     zs_sem, zr_sem, ys_sem, yr_sem,
@@ -185,7 +185,7 @@
         for r in range(2):
             start = r * (part_rows - 128)
             squares[i, u, tp, r:r + 1] = jnp.sum(folded[start:start + 128].T, axis=0, keepdims=True)
-        for k in range(1, tpn):
+        for k in range(2, tpn, 2):
             begin(move_sq(squares.at[i, u, tp], k, {"tp": lax.rem(tp + k, tpn)}))
         yield
         for side, h in ((0, 0), (1, 1), (0, 1), (1, 0)):
@@ -200,12 +200,19 @@
             part = ag_part(i, u, 2, h)
             move(part, 5 + h, partner).wait_recv()
             begin(move(part, 11 + h, partner))
-        yield
-        for k in range(1, tpn):
-            move_sq(squares.at[i, u, lax.rem(tp + tpn - k, tpn)], k, partner).wait_recv()
-        total = squares[i, u, 0]
-        for k in range(1, tpn):
-            total = total + squares[i, u, k]
+        total = squares[i, u, tp]
+        for k in range(2, tpn, 2):
+            there = lax.rem(tp + tpn - k, tpn)
+            move_sq(squares.at[i, u, there], k, partner).wait_recv()
+            total = total + squares[i, u, there]
+        core_sums[i, u, 0] = total
+        to_other = remote(
+            core_sums.at[i, u, 0], core_sums.at[i, u, 1], sqs_sem.at[i, u, 1], sqr_sem.at[i, u, 1], partner
+        )
+        begin(to_other)
+        yield
+        to_other.wait_recv()
+        total = core_sums[i, u, 0] + core_sums[i, u, 1]
         factor = lax.rsqrt(total * (1.0 / features) + EPS)
         tall = [jnp.broadcast_to(factor[r:r + 1], (128, 128)).T for r in range(2)]
         factors[i, u, :128] = tall[0]
@@ -375,13 +382,14 @@
         if step == half_n - 1:
             send_own(mix_ks)
         z_step(down_ks, step)
-        if step == 2:
+        if step == 4:
             y_wait_all(0)
             y_wait_all(1)
-        if step >= 2:
-            for u, t in todo[:2 if step in (3, 4) else 1]:
+        if step >= 4:
+            count = 2 if step == half_n else 1
+            for u, t in todo[:count]:
                 gu(0, u, t)
-            todo = todo[2 if step in (3, 4) else 1:]
+            todo = todo[count:]
     mix_steps = list(range(1, half_n + 1))
 
     def mix_step():
@@ -425,6 +433,7 @@
             vmem((n, 128, 128), BF16),
             vmem((3, 2, tpn, part, width), BF16),
             vmem((3, 2, tpn, 8, 128), F32),
+            vmem((3, 2, 2, 8, 128), F32),
             vmem((3, 2, part, 128), F32),
             vmem((rows, ff), BF16),
             vmem((2, part, third), F32),

time: 174 us -> 174 us (level)
  no operation moved by 1% of the time
where the time goes in v5:
time: 174 us; the launch traced here: 173 us
  Pallas kernels  171 us (98%)
    pallas_call x1, Pallas kernels, per_device(): pl.pallas_call(functools.partial(kernel, n), out_shape=jax.ShapeDtypeStru...  171 us

profile of v5, /device:TPU:33, one launch (start us, length us, event | category | flops | bytes accessed | tf_op | source)
XLA Modules:
  0.0 173.1 jit_solution(15199779320791024417)
XLA Ops:
  0.0 171.5 %shard_map.118 = bf16[384,256]{1,0:T(8,128)(2,1)} custom-call(bf16[384,256]{1,0:T(8,128)(2,1)} %x_hbm.1, bf16[1,256]{1,0:T(2,128)(2,1)} %g1_hbm.1, bf16[128,768]{1,0:T(8,128)(2,1)} %gate_hbm.1, bf16[128,768]{1,0:T(8,128)(2,1)} %up_hbm.1, bf16[768,128]{1,0:T(8,128)(2,1)} %down_hbm.1, bf16[1,256]{1,0:T(2,128)(2,1)} %gm_hbm.1, bf16[128,128]{1,0:T(8,128)(2,1)} %pin_hbm.1, ...), custom_call_target="tpu_custom_call" | custom-call | tf_op jit(solution)/shard_map/pallas_call | solution.py:420
  171.5 1.6 copy.14
